TPU v7x, 32 devices: a whole 2x2x4 slice. The times are simulated.
32 devices in a mesh: sp: 8 (over z, y), tp: 4 (over x, core).
Axes of the slice: x: 2, y: 2, z: 4, core: 2. Of those that a mesh axis runs over, the one named last changes fastest.
Arguments:
- tokens: bfloat16 [4, 3072, 2048], P(None, 'sp'), may hold values from -21 to 21
- query_weight: bfloat16 [2048, 1024], P(None, 'tp'), may hold values from -0.125 to 0.125
- key_weight: bfloat16 [2048, 1024], P(None, 'tp'), may hold values from -0.125 to 0.125
- value_weight: bfloat16 [2048, 1024], P(None, 'tp'), may hold values from -0.125 to 0.125
- out_gain: float32 [1024], replicated, may hold values from 0.1 to 1.9
- out_weight: bfloat16 [1024, 2048], P(None, 'tp'), may hold values from -0.1875 to 0.1875
Outputs:
- mixed_out: bfloat16 [4, 3072, 2048], P(None, 'sp', 'tp')
- total_log: float32 [4, 8, 3072], P(None, 'tp', 'sp')
All inputs are finite; a program needn't handle non-finite values.
Results may differ from a plain program's by a relative error of at most 0.0098.
Values may be sent and summed in bfloat16 or wider, within the bound.
A program may use at most 128 MiB of HBM per device.

v0:
```python
import functools
import math

import jax
import jax.numpy as jnp
from jax import lax
from jax.experimental import pallas as pl
from jax.experimental.pallas import tpu as pltpu
from jax.sharding import PartitionSpec as P

HEAD_DIM = 128
REACH = 64
FAR = 16
NEAR = 4
GRAN = FAR * FAR
ROPE_BASE = 10000.0
MASK_FILL = -1e30
NORM_FLOOR = 1e-06
LOG2E = 1.0 / math.log(2.0)
LN2 = math.log(2.0)
F32 = jnp.float32
BF16 = jnp.bfloat16

MESH = pl.DeviceIdType.MESH


def iota(shape, dim):
    return lax.broadcasted_iota(jnp.int32, shape, dim)


def perm_token(p):
    slot = p // FAR
    a = p % FAR
    residue = slot // NEAR + NEAR * (slot % (FAR // NEAR))
    return a * FAR + residue


def dot_t(a, b):
    return lax.dot_general(a, b, (((1,), (1,)), ((), ())), preferred_element_type=F32)


def layer_kernel(
    nsp, tok_h, wq_h, wk_h, wv_h, wo_h, cos_h, sin_h, gain, out, log_out,
    tok, wq, wk, wv, wo, cos, sin, kn, qn, kvs, qs, gath, outs, logs, lsend, lrow,
    kp, qp, mp, on, perm, bias1, bias4, bias16, o1, m1, l1,
    load_sem, send_sem, recv_sem,
):
    half = kn.shape[0]
    length = tok.shape[1]
    block = 2 * length
    grans = block // GRAN
    wide = REACH * FAR
    side = wide // GRAN
    tail = wide - block
    span = block + 2 * wide
    rows = block // FAR
    key_rows = span // FAR
    near_rows = rows + 2 * FAR
    cols = wq.shape[1]
    heads = cols // HEAD_DIM
    total = nsp * length
    scale = HEAD_DIM**-0.5 * LOG2E
    sp, t = lax.axis_index("sp"), lax.axis_index("tp")
    y, blk = sp % 2, sp // 2
    twin = sp + 1 - 2 * y
    x_peer = (t + 2) % 4
    d_peer = t + 1 - 2 * (t % 2)
    x_d_peer = (d_peer + 2) % 4
    mine, other = y * half, (1 - y) * half

    loads = []

    def load(src, dst):
        copy = pltpu.make_async_copy(src, dst, load_sem.at[len(loads)])
        copy.start()
        loads.append(copy)
        return copy

    got_wk, got_wv = load(wk_h, wk), load(wv_h, wv)
    got_tok = {("m", 0): load(tok_h.at[mine], tok.at[0])}
    got_cos, got_sin = load(cos_h, cos), load(sin_h, sin)
    got_tok["o", 0] = load(tok_h.at[other], tok.at[1])
    for s in range(1, half):
        got_tok["o", s] = load(tok_h.at[other + s], tok.at[2 * s + 1])
        got_tok["m", s] = load(tok_h.at[mine + s], tok.at[2 * s])
    got_wq, got_wo = load(wq_h, wq), load(wo_h, wo)

    barrier = pltpu.get_barrier_semaphore()
    has = {d: (sp + d >= 0) & (sp + d < nsp) for d in (2, -2, 4, -4)}
    for peer in ((twin, t), (sp, x_peer), (sp, d_peer)):
        pl.semaphore_signal(barrier, inc=1, device_id=peer, device_id_type=MESH)
    count = 3
    for d, there in has.items():
        count = count + there.astype(jnp.int32)

        @pl.when(there)
        def _(d=d):
            pl.semaphore_signal(barrier, inc=1, device_id=(sp + d, t), device_id_type=MESH)

    first = pl.multiple_of(y * length, HEAD_DIM)
    second = pl.multiple_of((1 - y) * length, HEAD_DIM)

    def clear(d, at, size):
        @pl.when(jnp.logical_not(has[d]))
        def _():
            for s in range(half):
                kn[s, at : at + size] = jnp.zeros((size, kn.shape[2]), BF16)

    clear(-4, 0, tail)
    clear(-2, tail, block)
    clear(2, wide + block, block)
    clear(4, span - tail, tail)

    numbers = {}

    def copy(name, src, dst, peer):
        n = numbers.setdefault(name, len(numbers))
        return pltpu.make_async_remote_copy(
            src_ref=src, dst_ref=dst, send_sem=send_sem.at[n], recv_sem=recv_sem.at[n],
            device_id=peer, device_id_type=MESH,
        )

    sent = []

    def start(c):
        c.start()
        sent.append((c, None))

    def z_copy(kind, s, d):
        peer = (sp + d, t)
        far = kind == "T"
        if far:
            src = wide + (block - tail if d > 0 else 0)
            dst = 0 if d > 0 else span - tail
            size = tail
        else:
            part = first if kind == "A" else second
            src = wide + part
            dst = (tail if d > 0 else wide + block) + part
            size = length
        return copy((kind, s, d), kn.at[s, pl.ds(src, size)], kn.at[s, pl.ds(dst, size)], peer)

    def z_start(kind, s):
        for d in (4, -4) if kind == "T" else (2, -2):
            c = z_copy(kind, s, d)

            @pl.when(has[d])
            def _():
                c.start()

            sent.append((c, has[d]))

    def z_wait(kind, s):
        for d in (4, -4) if kind == "T" else (2, -2):

            @pl.when(has[-d])
            def _():
                z_copy(kind, s, d).wait_recv()

    def turned(x, w, store):
        a = jnp.dot(x, w[...], preferred_element_type=F32)
        for h in range(heads):
            one = a[:, h * HEAD_DIM : (h + 1) * HEAD_DIM]
            store(h, (one * cos[...] + pltpu.roll(one, HEAD_DIM // 2, 1) * sin[...]).astype(BF16))

    def lanes(n):
        return slice(n * HEAD_DIM, (n + 1) * HEAD_DIM)

    def keys_values(x, put):
        turned(x, wk, lambda h, a: put(2 * h, a))
        v = jnp.dot(x, wv[...], preferred_element_type=F32).astype(BF16)
        for h in range(heads):
            put(2 * h + 1, v[:, lanes(h)])

    def own_kv(s):
        def put(n, a):
            kn[s, pl.ds(wide + first, length), lanes(n)] = a

        keys_values(tok[2 * s], put)

    def twin_kv(s):
        def put(n, a):
            kvs[s, :, lanes(n)] = a

        keys_values(tok[2 * s + 1], put)

    def own_q(s):
        def put(n, a):
            qn[s, pl.ds(first, length), lanes(n)] = a

        turned(tok[2 * s], wq, put)

    def twin_q(s):
        def put(n, a):
            qs[s, :, lanes(n)] = a

        turned(tok[2 * s + 1], wq, put)

    def y_kv(s, at):
        return copy(("yk", s), kvs.at[s], kn.at[s, pl.ds(wide + at, length)], (twin, t))

    def y_q(s, at):
        return copy(("yq", s), qs.at[s], qn.at[s, pl.ds(at, length)], (twin, t))

    for c in (got_wk, got_wv, got_cos, got_sin, got_tok["m", 0]):
        c.wait()
    own_kv(0)
    pl.semaphore_wait(barrier, count)
    z_start("A", 0)
    got_tok["o", 0].wait()
    twin_kv(0)
    start(y_kv(0, first))
    for s in range(1, half):
        got_tok["o", s].wait()
        got_tok["m", s].wait()
        twin_kv(s)
        start(y_kv(s, first))
        own_kv(s)
    got_wq.wait()
    for s in range(half):
        twin_q(s)
        own_q(s)
        if s == 0:
            y_kv(0, second).wait_recv()
            z_start("B", 0)
            z_start("T", 0)
        start(y_q(s, first))
    for s in range(1, half):
        z_start("A", s)
        y_kv(s, second).wait_recv()
        z_start("B", s)
        z_start("T", s)

    perm[...] = jnp.where(
        iota((GRAN, GRAN), 1) == perm_token(iota((GRAN, GRAN), 0)), 1.0, 0.0
    ).astype(BF16)
    origin = blk * block - wide
    shape = (GRAN, GRAN + 2 * REACH)
    token = perm_token(iota(shape, 0))
    for g in range(grans):
        q_at = wide + g * GRAN + token
        k_at = wide + g * GRAN - REACH + iota(shape, 1)
        ok = (jnp.abs(k_at - q_at) <= REACH) & (k_at + origin >= 0) & (k_at + origin < total)
        bias1[g] = jnp.where(ok, 0.0, MASK_FILL)
    per = FAR // NEAR
    shape = (per * rows, per * near_rows)
    row, col = iota(shape, 0), iota(shape, 1)
    q_at = (row % rows + side * FAR) * FAR + NEAR * (row // rows)
    k_at = (col % near_rows + (side - 1) * FAR) * FAR + NEAR * (col // near_rows)
    ok = (jnp.abs(k_at - q_at) <= REACH * NEAR) & (k_at + origin >= 0) & (k_at + origin < total)
    bias4[...] = jnp.where(ok, 0.0, MASK_FILL)
    shape = (rows, key_rows)
    q_at = iota(shape, 0) + side * FAR
    k_at = iota(shape, 1)
    ok = (
        (jnp.abs(k_at - q_at) <= REACH)
        & (k_at * FAR + origin >= 0)
        & (k_at * FAR + origin < total)
    )
    bias16[...] = jnp.where(ok, 0.0, MASK_FILL)

    def attend(s, h):
        kv_lanes = pl.ds(pl.multiple_of(h * 2 * HEAD_DIM, HEAD_DIM), 2 * HEAD_DIM)
        k_lanes = pl.ds(pl.multiple_of(h * 2 * HEAD_DIM, HEAD_DIM), HEAD_DIM)
        v_lanes = pl.ds(pl.multiple_of((h * 2 + 1) * HEAD_DIM, HEAD_DIM), HEAD_DIM)
        h_lanes = pl.ds(pl.multiple_of(h * HEAD_DIM, HEAD_DIM), HEAD_DIM)
        shuffle = perm[...]
        for j in range(span // GRAN):
            moved = jnp.dot(
                shuffle, kn[s, j * GRAN : (j + 1) * GRAN, kv_lanes], preferred_element_type=F32
            )
            kp[:, j * FAR : (j + 1) * FAR] = moved.astype(BF16).reshape(FAR, FAR, 2 * HEAD_DIM)
        for g in range(grans):
            moved = jnp.dot(
                shuffle, qn[s, g * GRAN : (g + 1) * GRAN, h_lanes], preferred_element_type=F32
            )
            moved = moved.astype(BF16)
            qp[:, g * FAR : (g + 1) * FAR] = moved.reshape(FAR, FAR, HEAD_DIM)
            at = wide + g * GRAN - REACH
            k = kn[s, at : at + GRAN + 2 * REACH, k_lanes]
            v = kn[s, at : at + GRAN + 2 * REACH, v_lanes]
            sc = dot_t(moved, k) * scale + bias1[g]
            m = jnp.max(sc, axis=1, keepdims=True)
            p = jnp.exp2(sc - m)
            l = jnp.sum(p, axis=1, keepdims=True)
            o = jnp.dot(p.astype(BF16), v, preferred_element_type=F32)
            cut = (FAR, FAR, HEAD_DIM)
            o1[:, g * FAR : (g + 1) * FAR] = o.reshape(cut)
            m1[:, g * FAR : (g + 1) * FAR] = jnp.broadcast_to(m, o.shape).reshape(cut)
            l1[:, g * FAR : (g + 1) * FAR] = jnp.broadcast_to(l, o.shape).reshape(cut)
        near_at = (side - 1) * FAR
        for group in range(NEAR):
            sel = slice(group * per, (group + 1) * per)
            flat = (per * rows, HEAD_DIM)
            q = qp[sel].reshape(flat)
            k4 = kp[sel, near_at : near_at + near_rows, :HEAD_DIM].reshape(-1, HEAD_DIM)
            v4 = kp[sel, near_at : near_at + near_rows, HEAD_DIM:].reshape(-1, HEAD_DIM)
            s4 = dot_t(q, k4) * scale + bias4[...]
            b16 = bias16[...]
            s16 = jnp.concatenate(
                [
                    dot_t(qp[group * per + i], kp[group * per + i, :, :HEAD_DIM]) * scale + b16
                    for i in range(per)
                ],
                axis=0,
            )
            m_old = m1[sel].reshape(flat)
            m_row = jnp.maximum(
                jnp.max(s4, axis=1, keepdims=True), jnp.max(s16, axis=1, keepdims=True)
            )
            m_new = jnp.maximum(m_old, m_row)
            m_col = m_new[:, :1]
            keep = jnp.exp2(m_old - m_new)
            p4 = jnp.exp2(s4 - m_col)
            p16 = jnp.exp2(s16 - m_col)
            l = l1[sel].reshape(flat) * keep + (
                jnp.sum(p4, axis=1, keepdims=True) + jnp.sum(p16, axis=1, keepdims=True)
            )
            p16 = p16.astype(BF16)
            o16 = jnp.concatenate(
                [
                    jnp.dot(
                        p16[i * rows : (i + 1) * rows],
                        kp[group * per + i, :, HEAD_DIM:],
                        preferred_element_type=F32,
                    )
                    for i in range(per)
                ],
                axis=0,
            )
            o = o1[sel].reshape(flat) * keep + o16
            o = o + jnp.dot(p4.astype(BF16), v4, preferred_element_type=F32)
            mp[sel] = (o / l).astype(BF16).reshape(per, rows, HEAD_DIM)
            m1[sel] = (m_new * LN2 + jnp.log(l)).reshape(per, rows, HEAD_DIM)
        lane = iota((GRAN, HEAD_DIM), 1)
        for g in range(grans):
            cut = slice(g * FAR, (g + 1) * FAR)
            back = lambda a: lax.dot_general(
                a, shuffle, (((0,), (0,)), ((), ())), preferred_element_type=F32
            )
            merged = lax.dot_general(
                shuffle,
                mp[:, cut].reshape(GRAN, HEAD_DIM),
                (((0,), (0,)), ((), ())),
                preferred_element_type=F32,
            )
            on[g * GRAN : (g + 1) * GRAN] = merged.astype(BF16)
            x = m1[:, cut].reshape(GRAN, HEAD_DIM)
            high = x.astype(BF16).astype(F32)
            mid = (x - high).astype(BF16).astype(F32)
            low = x - high - mid
            terms = jnp.where(
                lane == 0, high, jnp.where(lane == 1, mid, jnp.where(lane == 2, low, 0.0))
            )
            lrow[:, g * GRAN : (g + 1) * GRAN] = jnp.sum(
                back(terms.astype(BF16)), axis=0, keepdims=True
            )
        outs[s, :, h_lanes] = on[pl.ds(second, length)]
        gath[t, mine + s, :, h_lanes] = on[pl.ds(first, length)]
        logs[mine + s, pl.ds(h, 1)] = lrow[:, pl.ds(first, length)]
        lsend[s, pl.ds(h, 1)] = lrow[:, pl.ds(second, length)]

    def piece(name, s, owner, j, peer):
        return copy((name, s), gath.at[owner, j], gath.at[owner, j], peer)

    def finish(j):
        acc = None
        square = None
        for n in range(gath.shape[0]):
            x = gath[n, j].astype(F32)
            at = slice(n * cols, (n + 1) * cols)
            scaled = (x * gain[:, at]).astype(BF16)
            term = jnp.dot(scaled, wo[at], preferred_element_type=F32)
            sq = jnp.sum(x * x, axis=1, keepdims=True)
            acc = term if acc is None else acc + term
            square = sq if square is None else square + sq
        out[j] = (acc * lax.rsqrt(square / wo.shape[0] + NORM_FLOOR)).astype(BF16)

    for s in range(half):
        y_q(s, second).wait_recv()
        for kind in ("A", "B", "T"):
            z_wait(kind, s)

        def one(h, carry, s=s):
            attend(s, h)
            return carry

        lax.fori_loop(0, heads, one, 0)
        start(copy(("yo", s), outs.at[s], gath.at[t, mine + s], (twin, t)))
        start(piece("xm", s, t, mine + s, (sp, x_peer)))
        start(copy(("yl", s), lsend.at[s], logs.at[mine + s], (twin, t)))
        start(piece("dm", s, t, mine + s, (sp, d_peer)))
        copy(("yo", s), outs.at[s], gath.at[t, other + s], (twin, t)).wait_recv()
        start(piece("xr", s, t, other + s, (sp, x_peer)))
        start(piece("dr", s, t, other + s, (sp, d_peer)))
        if s == 0:
            got_wo.wait()
        piece("xm", s, x_peer, mine + s, (sp, x_peer)).wait_recv()
        start(piece("em", s, x_peer, mine + s, (sp, d_peer)))
        piece("dm", s, d_peer, mine + s, (sp, d_peer)).wait_recv()
        piece("em", s, x_d_peer, mine + s, (sp, d_peer)).wait_recv()
        finish(mine + s)
        piece("xr", s, x_peer, other + s, (sp, x_peer)).wait_recv()
        start(piece("er", s, x_peer, other + s, (sp, d_peer)))
        piece("dr", s, d_peer, other + s, (sp, d_peer)).wait_recv()
        piece("er", s, x_d_peer, other + s, (sp, d_peer)).wait_recv()
        finish(other + s)
        copy(("yl", s), lsend.at[s], logs.at[other + s], (twin, t)).wait_recv()
    log_out[...] = logs[...]
    for c, there in sent:
        if there is None:
            c.wait_send()
        else:

            @pl.when(there)
            def _(c=c):
                c.wait_send()


def layer(nsp, ntp, tokens, wq, wk, wv, wo, cos, sin, gain):
    seqs, length, width = tokens.shape
    half = seqs // 2
    cols = wq.shape[1]
    heads = cols // HEAD_DIM
    block = 2 * length
    wide = REACH * FAR
    span = block + 2 * wide
    rows = block // FAR
    near_rows = rows + 2 * FAR
    per = FAR // NEAR
    grans = block // GRAN
    hbm = pl.BlockSpec(memory_space=pl.ANY)
    vmem = pl.BlockSpec(memory_space=pltpu.VMEM)
    v = pltpu.VMEM
    return pl.pallas_call(
        functools.partial(layer_kernel, nsp),
        in_specs=[hbm] * 7 + [vmem],
        out_specs=[vmem, vmem],
        out_shape=[
            jax.ShapeDtypeStruct((seqs, length, wo.shape[1]), BF16),
            jax.ShapeDtypeStruct((seqs, heads, length), F32),
        ],
        scratch_shapes=[
            v(tokens.shape, BF16), v(wq.shape, BF16), v(wk.shape, BF16), v(wv.shape, BF16),
            v(wo.shape, BF16), v(cos.shape, F32), v(sin.shape, F32),
            v((half, span, 2 * cols), BF16),
            v((half, block, cols), BF16),
            v((half, length, 2 * cols), BF16),
            v((half, length, cols), BF16),
            v((ntp, seqs, length, cols), BF16),
            v((half, length, cols), BF16),
            v((seqs, heads, length), F32),
            v((half, heads, length), F32),
            v((1, block), F32),
            v((FAR, span // FAR, 2 * HEAD_DIM), BF16),
            v((FAR, rows, HEAD_DIM), BF16),
            v((FAR, rows, HEAD_DIM), BF16),
            v((block, HEAD_DIM), BF16),
            v((GRAN, GRAN), BF16),
            v((grans, GRAN, GRAN + 2 * REACH), F32),
            v((per * rows, per * near_rows), F32),
            v((rows, span // FAR), F32),
            v((FAR, rows, HEAD_DIM), F32),
            v((FAR, rows, HEAD_DIM), F32),
            v((FAR, rows, HEAD_DIM), F32),
            pltpu.SemaphoreType.DMA((seqs + 6,)),
            pltpu.SemaphoreType.DMA((16 * half,)),
            pltpu.SemaphoreType.DMA((16 * half,)),
        ],
        compiler_params=pltpu.CompilerParams(
            collective_id=0, has_side_effects=True, vmem_limit_bytes=56 * 2**20
        ),
        name="layer",
    )(tokens, wq, wk, wv, wo, cos, sin, gain)


def shards(tokens, query_weight, key_weight, value_weight, out_gain, out_weight):
    length = tokens.shape[1]
    sp = lax.axis_index("sp")
    half_dim = HEAD_DIM // 2
    frequency = ROPE_BASE ** (-jnp.arange(half_dim, dtype=F32) / half_dim)
    positions = sp * length + jnp.arange(length, dtype=jnp.int32)
    angles = positions.astype(F32)[:, None] * frequency[None, :]
    cos, sin = jnp.cos(angles), jnp.sin(angles)
    cos = jnp.concatenate([cos, cos], axis=1)
    sin = jnp.concatenate([-sin, sin], axis=1)
    return tuple(
        layer(
            lax.axis_size("sp"), lax.axis_size("tp"), tokens, query_weight, key_weight,
            value_weight, out_weight, cos, sin, out_gain[None, :],
        )
    )


def solution(mesh):
    return jax.shard_map(
        shards,
        mesh=mesh,
        in_specs=(
            P(None, "sp", None),
            P(None, "tp"),
            P(None, "tp"),
            P(None, "tp"),
            P(),
            P(None, "tp"),
        ),
        out_specs=(P(None, "sp", "tp"), P(None, "tp", "sp")),
        check_vma=False,
    )
```

profile of v0, /device:TPU:1, one launch (start us, length us, event | category | flops | bytes accessed | tf_op | source)
XLA Modules:
  0.0 94.0 jit_solution(12902889913327832935)
XLA Ops:
  0.7 0.8 fusion
  1.4 0.9 pad_maximum_fusion
  2.3 88.4 %layer.1 = (bf16[4,384,512]{2,1,0:T(8,128)(2,1)}, f32[4,2,384]{2,1,0:T(2,128)}) custom-call(bf16[4,384,2048]{2,1,0:T(8,128)(2,1)} %tok_h.1, bf16[2048,256]{1,0:T(8,128)(2,1)} %wq_h.1, bf16[2048,256]{1,0:T(8,128)(2,1)} %wk_h.1, bf16[2048,256]{1,0:T(8,128)(2,1)} %wv_h.1, bf16[1024,512]{1,0:T(8,128)(2,1)} %wo_h.1, f32[384,128]{1,0:T(8,128)} %get-tuple-element.5.cos_h, ...), custom_call_target="tpu_custom_call" | custom-call | tf_op jit(solution)/shard_map/layer/pallas_call | solution.py:435
  90.7 0.0 copy-start
  90.7 2.7 %copy.10 = bf16[4,384,512]{2,1,0:T(8,128)(2,1)} copy(bf16[4,384,512]{2,1,0:T(8,128)(2,1)} %get-tuple-element.9) | data formatting | bytes 3145728
  93.4 0.0 copy-done
  93.4 0.6 copy.11
  (2 shorter events, 0.0 us)
Async XLA Ops:
  90.7 2.7 %copy-start = (f32[4,2,384]{2,1,0:T(2,128)S(1)}, f32[4,2,384]{2,1,0:T(2,128)}, u32[]{:S(2)}) copy-start(f32[4,2,384]{2,1,0:T(2,128)} %get-tuple-element.10) | copy-start | bytes 36868
where the time goes:
time: 94.2 us; the launch traced here: 94 us
  Pallas kernels  88.4 us (94%)
  local copies, waits for them, and re-layouts  3.26 us (3%)
  other arithmetic  1.69 us (2%)
    pallas_call x1, Pallas kernels, layer(): pl.pallas_call(functools.partial(layer_kernel, nsp), in_specs=[hbm] * 7 +...  88.4 us
    unnamed x4, local copies, waits for them, and re-layouts  3.26 us

commit v1 on v0

--- a/solution.py
+++ b/solution.py
@@ -45,7 +45,8 @@
     kp, qp, mp, on, perm, bias1, bias4, bias16, o1, m1, l1,
     load_sem, send_sem, recv_sem,
 ):
-    half = kn.shape[0]
+    half = tok.shape[0] // 2
+    units = kn.shape[0]
     length = tok.shape[1]
     block = 2 * length
     grans = block // GRAN
@@ -87,10 +88,12 @@
 
     barrier = pltpu.get_barrier_semaphore()
     has = {d: (sp + d >= 0) & (sp + d < nsp) for d in (2, -2, 4, -4)}
+    reach = {d: has[d] & has[-d] for d in (2, -2)}
     for peer in ((twin, t), (sp, x_peer), (sp, d_peer)):
         pl.semaphore_signal(barrier, inc=1, device_id=peer, device_id_type=MESH)
     count = 3
-    for d, there in has.items():
+    for d in (2, -2):
+        there = has[d]
         count = count + there.astype(jnp.int32)
 
         @pl.when(there)
@@ -103,8 +106,8 @@
     def clear(d, at, size):
         @pl.when(jnp.logical_not(has[d]))
         def _():
-            for s in range(half):
-                kn[s, at : at + size] = jnp.zeros((size, kn.shape[2]), BF16)
+            for u in range(units):
+                kn[u, at : at + size] = jnp.zeros((size, kn.shape[2]), BF16)
 
     clear(-4, 0, tail)
     clear(-2, tail, block)
@@ -126,11 +129,9 @@
         c.start()
         sent.append((c, None))
 
-    def z_copy(kind, s, d):
-        peer = (sp + d, t)
-        far = kind == "T"
-        if far:
-            src = wide + (block - tail if d > 0 else 0)
+    def z_copy(kind, u, d):
+        if kind == "T":
+            src = wide - tail if d > 0 else wide + block
             dst = 0 if d > 0 else span - tail
             size = tail
         else:
@@ -138,24 +139,27 @@
             src = wide + part
             dst = (tail if d > 0 else wide + block) + part
             size = length
-        return copy((kind, s, d), kn.at[s, pl.ds(src, size)], kn.at[s, pl.ds(dst, size)], peer)
-
-    def z_start(kind, s):
-        for d in (4, -4) if kind == "T" else (2, -2):
-            c = z_copy(kind, s, d)
-
-            @pl.when(has[d])
+        return copy(
+            (kind, u, d), kn.at[u, pl.ds(src, size)], kn.at[u, pl.ds(dst, size)], (sp + d, t)
+        )
+
+    def z_start(kind, u):
+        for d in (2, -2):
+            c = z_copy(kind, u, d)
+            there = reach[d] if kind == "T" else has[d]
+
+            @pl.when(there)
             def _():
                 c.start()
 
-            sent.append((c, has[d]))
-
-    def z_wait(kind, s):
-        for d in (4, -4) if kind == "T" else (2, -2):
-
-            @pl.when(has[-d])
+            sent.append((c, there))
+
+    def z_wait(kind, u):
+        for d in (2, -2):
+
+            @pl.when(has[-2 * d] if kind == "T" else has[-d])
             def _():
-                z_copy(kind, s, d).wait_recv()
+                z_copy(kind, u, d).wait_recv()
 
     def turned(x, w, store):
         a = jnp.dot(x, w[...], preferred_element_type=F32)
@@ -174,62 +178,68 @@
 
     def own_kv(s):
         def put(n, a):
-            kn[s, pl.ds(wide + first, length), lanes(n)] = a
+            kn[s * heads + n // 2, pl.ds(wide + first, length), lanes(n % 2)] = a
 
         keys_values(tok[2 * s], put)
 
     def twin_kv(s):
         def put(n, a):
-            kvs[s, :, lanes(n)] = a
+            kvs[s * heads + n // 2, :, lanes(n % 2)] = a
 
         keys_values(tok[2 * s + 1], put)
 
     def own_q(s):
         def put(n, a):
-            qn[s, pl.ds(first, length), lanes(n)] = a
+            qn[s * heads + n, pl.ds(first, length)] = a
 
         turned(tok[2 * s], wq, put)
 
     def twin_q(s):
         def put(n, a):
-            qs[s, :, lanes(n)] = a
+            qs[s * heads + n] = a
 
         turned(tok[2 * s + 1], wq, put)
 
-    def y_kv(s, at):
-        return copy(("yk", s), kvs.at[s], kn.at[s, pl.ds(wide + at, length)], (twin, t))
-
-    def y_q(s, at):
-        return copy(("yq", s), qs.at[s], qn.at[s, pl.ds(at, length)], (twin, t))
+    def y_kv(u, at):
+        return copy(("yk", u), kvs.at[u], kn.at[u, pl.ds(wide + at, length)], (twin, t))
+
+    def y_q(u, at):
+        return copy(("yq", u), qs.at[u], qn.at[u, pl.ds(at, length)], (twin, t))
+
+    def of(s):
+        return range(s * heads, (s + 1) * heads)
 
     for c in (got_wk, got_wv, got_cos, got_sin, got_tok["m", 0]):
         c.wait()
     own_kv(0)
     pl.semaphore_wait(barrier, count)
-    z_start("A", 0)
+    for u in of(0):
+        z_start("A", u)
     got_tok["o", 0].wait()
     twin_kv(0)
-    start(y_kv(0, first))
+    for u in of(0):
+        start(y_kv(u, first))
     for s in range(1, half):
         got_tok["o", s].wait()
         got_tok["m", s].wait()
         twin_kv(s)
-        start(y_kv(s, first))
+        for u in of(s):
+            start(y_kv(u, first))
         own_kv(s)
+    y_kv(0, second).wait_recv()
+    z_start("B", 0)
     got_wq.wait()
-    for s in range(half):
+    twin_q(0)
+    own_q(0)
+    for u in of(0):
+        start(y_q(u, first))
+    y_kv(1, second).wait_recv()
+    z_start("B", 1)
+    for s in range(1, half):
         twin_q(s)
         own_q(s)
-        if s == 0:
-            y_kv(0, second).wait_recv()
-            z_start("B", 0)
-            z_start("T", 0)
-        start(y_q(s, first))
-    for s in range(1, half):
-        z_start("A", s)
-        y_kv(s, second).wait_recv()
-        z_start("B", s)
-        z_start("T", s)
+        for u in of(s):
+            start(y_q(u, first))
 
     perm[...] = jnp.where(
         iota((GRAN, GRAN), 1) == perm_token(iota((GRAN, GRAN), 0)), 1.0, 0.0
@@ -259,52 +269,62 @@
     )
     bias16[...] = jnp.where(ok, 0.0, MASK_FILL)
 
-    def attend(s, h):
-        kv_lanes = pl.ds(pl.multiple_of(h * 2 * HEAD_DIM, HEAD_DIM), 2 * HEAD_DIM)
-        k_lanes = pl.ds(pl.multiple_of(h * 2 * HEAD_DIM, HEAD_DIM), HEAD_DIM)
-        v_lanes = pl.ds(pl.multiple_of((h * 2 + 1) * HEAD_DIM, HEAD_DIM), HEAD_DIM)
-        h_lanes = pl.ds(pl.multiple_of(h * HEAD_DIM, HEAD_DIM), HEAD_DIM)
-        shuffle = perm[...]
-        for j in range(span // GRAN):
+    def gather_keys(u, slot, chunks):
+        for j in chunks:
             moved = jnp.dot(
-                shuffle, kn[s, j * GRAN : (j + 1) * GRAN, kv_lanes], preferred_element_type=F32
-            )
-            kp[:, j * FAR : (j + 1) * FAR] = moved.astype(BF16).reshape(FAR, FAR, 2 * HEAD_DIM)
+                perm[...], kn[u, j * GRAN : (j + 1) * GRAN], preferred_element_type=F32
+            )
+            moved = moved.astype(BF16).reshape(FAR, FAR, 2 * HEAD_DIM)
+            kp[slot, :, j * FAR : (j + 1) * FAR] = moved
+
+    ends = tail // GRAN
+
+    def attend_close(u):
+        slot = u % 2
+        y_q(u, second).wait_recv()
+        gather_keys(u, slot, range(ends, span // GRAN - ends))
         for g in range(grans):
             moved = jnp.dot(
-                shuffle, qn[s, g * GRAN : (g + 1) * GRAN, h_lanes], preferred_element_type=F32
+                perm[...], qn[u, g * GRAN : (g + 1) * GRAN], preferred_element_type=F32
             )
             moved = moved.astype(BF16)
-            qp[:, g * FAR : (g + 1) * FAR] = moved.reshape(FAR, FAR, HEAD_DIM)
+            qp[slot, :, g * FAR : (g + 1) * FAR] = moved.reshape(FAR, FAR, HEAD_DIM)
             at = wide + g * GRAN - REACH
-            k = kn[s, at : at + GRAN + 2 * REACH, k_lanes]
-            v = kn[s, at : at + GRAN + 2 * REACH, v_lanes]
+            k = kn[u, at : at + GRAN + 2 * REACH, :HEAD_DIM]
+            v = kn[u, at : at + GRAN + 2 * REACH, HEAD_DIM:]
             sc = dot_t(moved, k) * scale + bias1[g]
             m = jnp.max(sc, axis=1, keepdims=True)
             p = jnp.exp2(sc - m)
             l = jnp.sum(p, axis=1, keepdims=True)
             o = jnp.dot(p.astype(BF16), v, preferred_element_type=F32)
             cut = (FAR, FAR, HEAD_DIM)
-            o1[:, g * FAR : (g + 1) * FAR] = o.reshape(cut)
-            m1[:, g * FAR : (g + 1) * FAR] = jnp.broadcast_to(m, o.shape).reshape(cut)
-            l1[:, g * FAR : (g + 1) * FAR] = jnp.broadcast_to(l, o.shape).reshape(cut)
+            o1[slot, :, g * FAR : (g + 1) * FAR] = o.reshape(cut)
+            m1[slot, :, g * FAR : (g + 1) * FAR] = jnp.broadcast_to(m, o.shape).reshape(cut)
+            l1[slot, :, g * FAR : (g + 1) * FAR] = jnp.broadcast_to(l, o.shape).reshape(cut)
+
+    def attend_far(u):
+        slot = u % 2
+        s, h = u // heads, u % heads
+        z_wait("T", u)
+        gather_keys(u, slot, [*range(ends), *range(span // GRAN - ends, span // GRAN)])
+        shuffle = perm[...]
         near_at = (side - 1) * FAR
         for group in range(NEAR):
             sel = slice(group * per, (group + 1) * per)
             flat = (per * rows, HEAD_DIM)
-            q = qp[sel].reshape(flat)
-            k4 = kp[sel, near_at : near_at + near_rows, :HEAD_DIM].reshape(-1, HEAD_DIM)
-            v4 = kp[sel, near_at : near_at + near_rows, HEAD_DIM:].reshape(-1, HEAD_DIM)
+            q = qp[slot, sel].reshape(flat)
+            k4 = kp[slot, sel, near_at : near_at + near_rows, :HEAD_DIM].reshape(-1, HEAD_DIM)
+            v4 = kp[slot, sel, near_at : near_at + near_rows, HEAD_DIM:].reshape(-1, HEAD_DIM)
             s4 = dot_t(q, k4) * scale + bias4[...]
             b16 = bias16[...]
             s16 = jnp.concatenate(
                 [
-                    dot_t(qp[group * per + i], kp[group * per + i, :, :HEAD_DIM]) * scale + b16
+                    dot_t(qp[slot, group * per + i], kp[slot, group * per + i, :, :HEAD_DIM]) * scale + b16
                     for i in range(per)
                 ],
                 axis=0,
             )
-            m_old = m1[sel].reshape(flat)
+            m_old = m1[slot, sel].reshape(flat)
             m_row = jnp.maximum(
                 jnp.max(s4, axis=1, keepdims=True), jnp.max(s16, axis=1, keepdims=True)
             )
@@ -313,7 +333,7 @@
             keep = jnp.exp2(m_old - m_new)
             p4 = jnp.exp2(s4 - m_col)
             p16 = jnp.exp2(s16 - m_col)
-            l = l1[sel].reshape(flat) * keep + (
+            l = l1[slot, sel].reshape(flat) * keep + (
                 jnp.sum(p4, axis=1, keepdims=True) + jnp.sum(p16, axis=1, keepdims=True)
             )
             p16 = p16.astype(BF16)
@@ -321,17 +341,17 @@
                 [
                     jnp.dot(
                         p16[i * rows : (i + 1) * rows],
-                        kp[group * per + i, :, HEAD_DIM:],
+                        kp[slot, group * per + i, :, HEAD_DIM:],
                         preferred_element_type=F32,
                     )
                     for i in range(per)
                 ],
                 axis=0,
             )
-            o = o1[sel].reshape(flat) * keep + o16
+            o = o1[slot, sel].reshape(flat) * keep + o16
             o = o + jnp.dot(p4.astype(BF16), v4, preferred_element_type=F32)
             mp[sel] = (o / l).astype(BF16).reshape(per, rows, HEAD_DIM)
-            m1[sel] = (m_new * LN2 + jnp.log(l)).reshape(per, rows, HEAD_DIM)
+            m1[slot, sel] = (m_new * LN2 + jnp.log(l)).reshape(per, rows, HEAD_DIM)
         lane = iota((GRAN, HEAD_DIM), 1)
         for g in range(grans):
             cut = slice(g * FAR, (g + 1) * FAR)
@@ -345,7 +365,7 @@
                 preferred_element_type=F32,
             )
             on[g * GRAN : (g + 1) * GRAN] = merged.astype(BF16)
-            x = m1[:, cut].reshape(GRAN, HEAD_DIM)
+            x = m1[slot, :, cut].reshape(GRAN, HEAD_DIM)
             high = x.astype(BF16).astype(F32)
             mid = (x - high).astype(BF16).astype(F32)
             low = x - high - mid
@@ -355,19 +375,44 @@
             lrow[:, g * GRAN : (g + 1) * GRAN] = jnp.sum(
                 back(terms.astype(BF16)), axis=0, keepdims=True
             )
-        outs[s, :, h_lanes] = on[pl.ds(second, length)]
-        gath[t, mine + s, :, h_lanes] = on[pl.ds(first, length)]
-        logs[mine + s, pl.ds(h, 1)] = lrow[:, pl.ds(first, length)]
-        lsend[s, pl.ds(h, 1)] = lrow[:, pl.ds(second, length)]
-
-    def piece(name, s, owner, j, peer):
-        return copy((name, s), gath.at[owner, j], gath.at[owner, j], peer)
+        outs[u] = on[pl.ds(second, length)]
+        gath[t, mine + s, h] = on[pl.ds(first, length)]
+        logs[mine + s, h] = lrow[:, pl.ds(first, length)]
+        lsend[u] = lrow[:, pl.ds(second, length)]
+        start(across(u, mine))
+        start(piece("xm", u, t, mine, (sp, x_peer)))
+        start(piece("dm", u, t, mine, (sp, d_peer)))
+        start(log_across(u, mine))
+
+    def across(u, base):
+        return copy(
+            ("yo", u), outs.at[u], gath.at[t, base + u // heads, u % heads], (twin, t)
+        )
+
+    def log_across(u, base):
+        return copy(("yl", u), lsend.at[u], logs.at[base + u // heads, u % heads], (twin, t))
+
+    def piece(name, u, owner, base, peer):
+        ref = gath.at[owner, base + u // heads, u % heads]
+        return copy((name, u), ref, ref, peer)
+
+    def spread(u):
+        across(u, other).wait_recv()
+        start(piece("xr", u, t, other, (sp, x_peer)))
+        start(piece("dr", u, t, other, (sp, d_peer)))
+        piece("xm", u, x_peer, mine, (sp, x_peer)).wait_recv()
+        start(piece("em", u, x_peer, mine, (sp, d_peer)))
+
+    def spread_twin(u):
+        piece("xr", u, x_peer, other, (sp, x_peer)).wait_recv()
+        start(piece("er", u, x_peer, other, (sp, d_peer)))
+        log_across(u, other).wait_recv()
 
     def finish(j):
         acc = None
         square = None
         for n in range(gath.shape[0]):
-            x = gath[n, j].astype(F32)
+            x = jnp.concatenate([gath[n, j, h] for h in range(heads)], axis=1).astype(F32)
             at = slice(n * cols, (n + 1) * cols)
             scaled = (x * gain[:, at]).astype(BF16)
             term = jnp.dot(scaled, wo[at], preferred_element_type=F32)
@@ -376,37 +421,60 @@
             square = sq if square is None else square + sq
         out[j] = (acc * lax.rsqrt(square / wo.shape[0] + NORM_FLOOR)).astype(BF16)
 
-    for s in range(half):
-        y_q(s, second).wait_recv()
-        for kind in ("A", "B", "T"):
-            z_wait(kind, s)
-
-        def one(h, carry, s=s):
-            attend(s, h)
-            return carry
-
-        lax.fori_loop(0, heads, one, 0)
-        start(copy(("yo", s), outs.at[s], gath.at[t, mine + s], (twin, t)))
-        start(piece("xm", s, t, mine + s, (sp, x_peer)))
-        start(copy(("yl", s), lsend.at[s], logs.at[mine + s], (twin, t)))
-        start(piece("dm", s, t, mine + s, (sp, d_peer)))
-        copy(("yo", s), outs.at[s], gath.at[t, other + s], (twin, t)).wait_recv()
-        start(piece("xr", s, t, other + s, (sp, x_peer)))
-        start(piece("dr", s, t, other + s, (sp, d_peer)))
-        if s == 0:
-            got_wo.wait()
-        piece("xm", s, x_peer, mine + s, (sp, x_peer)).wait_recv()
-        start(piece("em", s, x_peer, mine + s, (sp, d_peer)))
-        piece("dm", s, d_peer, mine + s, (sp, d_peer)).wait_recv()
-        piece("em", s, x_d_peer, mine + s, (sp, d_peer)).wait_recv()
+    def finish_mine(s):
+        for u in of(s):
+            piece("dm", u, d_peer, mine, (sp, d_peer)).wait_recv()
+            piece("em", u, x_d_peer, mine, (sp, d_peer)).wait_recv()
         finish(mine + s)
-        piece("xr", s, x_peer, other + s, (sp, x_peer)).wait_recv()
-        start(piece("er", s, x_peer, other + s, (sp, d_peer)))
-        piece("dr", s, d_peer, other + s, (sp, d_peer)).wait_recv()
-        piece("er", s, x_d_peer, other + s, (sp, d_peer)).wait_recv()
+
+    def finish_other(s):
+        for u in of(s):
+            piece("dr", u, d_peer, other, (sp, d_peer)).wait_recv()
+            piece("er", u, x_d_peer, other, (sp, d_peer)).wait_recv()
         finish(other + s)
-        copy(("yl", s), lsend.at[s], logs.at[other + s], (twin, t)).wait_recv()
-    log_out[...] = logs[...]
+
+    def arrived(u):
+        z_wait("A", u)
+        z_wait("B", u)
+
+    arrived(0)
+    z_start("T", 0)
+    z_start("A", 2)
+    arrived(1)
+    z_start("T", 1)
+    y_kv(2, second).wait_recv()
+    z_start("B", 2)
+    z_start("A", 3)
+    attend_close(0)
+    attend_far(0)
+    attend_close(1)
+    attend_far(1)
+    arrived(2)
+    z_start("T", 2)
+    y_kv(3, second).wait_recv()
+    z_start("B", 3)
+    spread(0)
+    spread(1)
+    attend_close(2)
+    spread_twin(0)
+    spread_twin(1)
+    got_wo.wait()
+    arrived(3)
+    z_start("T", 3)
+    attend_close(3)
+    attend_far(2)
+    finish_mine(0)
+    spread(2)
+    attend_far(3)
+    spread_twin(2)
+    finish_other(0)
+    spread(3)
+    finish_mine(1)
+    spread_twin(3)
+    finish_other(1)
+    for j in range(logs.shape[0]):
+        for h in range(heads):
+            log_out[j, h : h + 1] = logs[j, h]
     for c, there in sent:
         if there is None:
             c.wait_send()
@@ -443,29 +511,29 @@
         scratch_shapes=[
             v(tokens.shape, BF16), v(wq.shape, BF16), v(wk.shape, BF16), v(wv.shape, BF16),
             v(wo.shape, BF16), v(cos.shape, F32), v(sin.shape, F32),
-            v((half, span, 2 * cols), BF16),
-            v((half, block, cols), BF16),
-            v((half, length, 2 * cols), BF16),
-            v((half, length, cols), BF16),
-            v((ntp, seqs, length, cols), BF16),
-            v((half, length, cols), BF16),
-            v((seqs, heads, length), F32),
-            v((half, heads, length), F32),
+            v((half * heads, span, 2 * HEAD_DIM), BF16),
+            v((half * heads, block, HEAD_DIM), BF16),
+            v((half * heads, length, 2 * HEAD_DIM), BF16),
+            v((half * heads, length, HEAD_DIM), BF16),
+            v((ntp, seqs, heads, length, HEAD_DIM), BF16),
+            v((half * heads, length, HEAD_DIM), BF16),
+            v((seqs, heads, 1, length), F32),
+            v((half * heads, 1, length), F32),
             v((1, block), F32),
-            v((FAR, span // FAR, 2 * HEAD_DIM), BF16),
-            v((FAR, rows, HEAD_DIM), BF16),
+            v((2, FAR, span // FAR, 2 * HEAD_DIM), BF16),
+            v((2, FAR, rows, HEAD_DIM), BF16),
             v((FAR, rows, HEAD_DIM), BF16),
             v((block, HEAD_DIM), BF16),
             v((GRAN, GRAN), BF16),
             v((grans, GRAN, GRAN + 2 * REACH), F32),
             v((per * rows, per * near_rows), F32),
             v((rows, span // FAR), F32),
-            v((FAR, rows, HEAD_DIM), F32),
-            v((FAR, rows, HEAD_DIM), F32),
-            v((FAR, rows, HEAD_DIM), F32),
+            v((2, FAR, rows, HEAD_DIM), F32),
+            v((2, FAR, rows, HEAD_DIM), F32),
+            v((2, FAR, rows, HEAD_DIM), F32),
             pltpu.SemaphoreType.DMA((seqs + 6,)),
-            pltpu.SemaphoreType.DMA((16 * half,)),
-            pltpu.SemaphoreType.DMA((16 * half,)),
+            pltpu.SemaphoreType.DMA((16 * half * heads,)),
+            pltpu.SemaphoreType.DMA((16 * half * heads,)),
         ],
         compiler_params=pltpu.CompilerParams(
             collective_id=0, has_side_effects=True, vmem_limit_bytes=56 * 2**20

time: 94.2 us -> 77.8 us (0.83)
  Pallas kernels: 88.4 us -> 72 us
    pallas_call x1, Pallas kernels: 88.4 us -> 72 us  [layer(): pl.pallas_call(functools.partial(layer_kernel, nsp), in_specs=[hbm] * 7 +...]
where the time goes in v1:
time: 77.8 us; the launch traced here: 77.7 us
  Pallas kernels  72 us (93%)
  local copies, waits for them, and re-layouts  3.26 us (4%)
  other arithmetic  1.69 us (2%)
    pallas_call x1, Pallas kernels, layer(): pl.pallas_call(functools.partial(layer_kernel, nsp), in_specs=[hbm] * 7 +...  72 us
    unnamed x4, local copies, waits for them, and re-layouts  3.26 us

profile of v1, /device:TPU:1, one launch (start us, length us, event | category | flops | bytes accessed | tf_op | source)
XLA Modules:
  0.0 77.7 jit_solution(3533514085429829441)
XLA Ops:
  0.7 0.8 fusion
  1.4 0.9 %pad_maximum_fusion = (f32[384,128]{1,0:T(8,128)}, f32[384,128]{1,0:T(8,128)}) fusion(f32[384,64]{1,0:T(8,128)S(1)} %get-tuple-element.4, f32[384,64]{1,0:T(8,128)S(1)} %get-tuple-element.3, f32[384,64]{1,0:T(8,128)S(1)} %get-tuple-element.2), kind=kLoop, calls=%fused_computation.2 | loop fusion | flops 98304 | bytes 688128 | tf_op jit(solution)/shard_map/concatenate | solution.py:553
  2.3 72.0 %layer.1 = (bf16[4,384,512]{2,1,0:T(8,128)(2,1)}, f32[4,2,384]{2,1,0:T(2,128)}) custom-call(bf16[4,384,2048]{2,1,0:T(8,128)(2,1)} %tok_h.1, bf16[2048,256]{1,0:T(8,128)(2,1)} %wq_h.1, bf16[2048,256]{1,0:T(8,128)(2,1)} %wk_h.1, bf16[2048,256]{1,0:T(8,128)(2,1)} %wv_h.1, bf16[1024,512]{1,0:T(8,128)(2,1)} %wo_h.1, f32[384,128]{1,0:T(8,128)} %get-tuple-element.5.cos_h, ...), custom_call_target="tpu_custom_call" | custom-call | tf_op jit(solution)/shard_map/layer/pallas_call | solution.py:503
  74.4 0.0 copy-start
  74.4 2.7 %copy.10 = bf16[4,384,512]{2,1,0:T(8,128)(2,1)} copy(bf16[4,384,512]{2,1,0:T(8,128)(2,1)} %get-tuple-element.9) | data formatting | bytes 3145728
  77.1 0.0 copy-done
  77.1 0.6 copy.11
  (2 shorter events, 0.0 us)
Async XLA Ops:
  74.4 2.7 %copy-start = (f32[4,2,384]{2,1,0:T(2,128)S(1)}, f32[4,2,384]{2,1,0:T(2,128)}, u32[]{:S(2)}) copy-start(f32[4,2,384]{2,1,0:T(2,128)} %get-tuple-element.10) | copy-start | bytes 36868

commit v2 on v1

--- a/solution.py
+++ b/solution.py
@@ -3,6 +3,7 @@
 
 import jax
 import jax.numpy as jnp
+import numpy as np
 from jax import lax
 from jax.experimental import pallas as pl
 from jax.experimental.pallas import tpu as pltpu
@@ -40,7 +41,8 @@
 
 
 def layer_kernel(
-    nsp, tok_h, wq_h, wk_h, wv_h, wo_h, cos_h, sin_h, gain, out, log_out,
+    nsp, tok_h, wq_h, wk_h, wv_h, wo_h, cos_h, sin_h, cos_base, sin_base, gain,
+    out, log_out,
     tok, wq, wk, wv, wo, cos, sin, kn, qn, kvs, qs, gath, outs, logs, lsend, lrow,
     kp, qp, mp, on, perm, bias1, bias4, bias16, o1, m1, l1,
     load_sem, send_sem, recv_sem,
@@ -77,14 +79,9 @@
         loads.append(copy)
         return copy
 
+    got_cos, got_sin = load(cos_h, cos), load(sin_h, sin)
     got_wk, got_wv = load(wk_h, wk), load(wv_h, wv)
     got_tok = {("m", 0): load(tok_h.at[mine], tok.at[0])}
-    got_cos, got_sin = load(cos_h, cos), load(sin_h, sin)
-    got_tok["o", 0] = load(tok_h.at[other], tok.at[1])
-    for s in range(1, half):
-        got_tok["o", s] = load(tok_h.at[other + s], tok.at[2 * s + 1])
-        got_tok["m", s] = load(tok_h.at[mine + s], tok.at[2 * s])
-    got_wq, got_wo = load(wq_h, wq), load(wo_h, wo)
 
     barrier = pltpu.get_barrier_semaphore()
     has = {d: (sp + d >= 0) & (sp + d < nsp) for d in (2, -2, 4, -4)}
@@ -209,16 +206,33 @@
     def of(s):
         return range(s * heads, (s + 1) * heads)
 
-    for c in (got_wk, got_wv, got_cos, got_sin, got_tok["m", 0]):
+    cos_at, sin_at = cos_base[pl.ds(sp, 1)], sin_base[pl.ds(sp, 1)]
+    sign = jnp.where(iota(cos.shape, 1) < HEAD_DIM // 2, -1.0, 1.0)
+    got_cos.wait()
+    got_sin.wait()
+    cos_step, sin_step = cos[...], sin[...]
+    cos[...] = cos_step * cos_at - sin_step * sin_at
+    sin[...] = (sin_step * cos_at + cos_step * sin_at) * sign
+    for c in (got_wk, got_wv, got_tok["m", 0]):
         c.wait()
+    got_tok["o", 0] = load(tok_h.at[other], tok.at[1])
     own_kv(0)
     pl.semaphore_wait(barrier, count)
     for u in of(0):
         z_start("A", u)
     got_tok["o", 0].wait()
+    got_wq = load(wq_h, wq)
+    for s in range(1, half):
+        got_tok["o", s] = load(tok_h.at[other + s], tok.at[2 * s + 1])
+        got_tok["m", s] = load(tok_h.at[mine + s], tok.at[2 * s])
+    got_wo = load(wo_h, wo)
     twin_kv(0)
     for u in of(0):
         start(y_kv(u, first))
+    got_wq.wait()
+    twin_q(0)
+    for u in of(0):
+        start(y_q(u, first))
     for s in range(1, half):
         got_tok["o", s].wait()
         got_tok["m", s].wait()
@@ -228,11 +242,7 @@
         own_kv(s)
     y_kv(0, second).wait_recv()
     z_start("B", 0)
-    got_wq.wait()
-    twin_q(0)
     own_q(0)
-    for u in of(0):
-        start(y_q(u, first))
     y_kv(1, second).wait_recv()
     z_start("B", 1)
     for s in range(1, half):
@@ -485,7 +495,7 @@
                 c.wait_send()
 
 
-def layer(nsp, ntp, tokens, wq, wk, wv, wo, cos, sin, gain):
+def layer(nsp, ntp, tokens, wq, wk, wv, wo, tables, gain):
     seqs, length, width = tokens.shape
     half = seqs // 2
     cols = wq.shape[1]
@@ -502,7 +512,7 @@
     v = pltpu.VMEM
     return pl.pallas_call(
         functools.partial(layer_kernel, nsp),
-        in_specs=[hbm] * 7 + [vmem],
+        in_specs=[hbm] * 7 + [vmem] * 3,
         out_specs=[vmem, vmem],
         out_shape=[
             jax.ShapeDtypeStruct((seqs, length, wo.shape[1]), BF16),
@@ -510,7 +520,7 @@
         ],
         scratch_shapes=[
             v(tokens.shape, BF16), v(wq.shape, BF16), v(wk.shape, BF16), v(wv.shape, BF16),
-            v(wo.shape, BF16), v(cos.shape, F32), v(sin.shape, F32),
+            v(wo.shape, BF16), v((length, HEAD_DIM), F32), v((length, HEAD_DIM), F32),
             v((half * heads, span, 2 * HEAD_DIM), BF16),
             v((half * heads, block, HEAD_DIM), BF16),
             v((half * heads, length, 2 * HEAD_DIM), BF16),
@@ -539,23 +549,23 @@
             collective_id=0, has_side_effects=True, vmem_limit_bytes=56 * 2**20
         ),
         name="layer",
-    )(tokens, wq, wk, wv, wo, cos, sin, gain)
+    )(tokens, wq, wk, wv, wo, *tables, gain)
 
 
 def shards(tokens, query_weight, key_weight, value_weight, out_gain, out_weight):
     length = tokens.shape[1]
-    sp = lax.axis_index("sp")
-    half_dim = HEAD_DIM // 2
-    frequency = ROPE_BASE ** (-jnp.arange(half_dim, dtype=F32) / half_dim)
-    positions = sp * length + jnp.arange(length, dtype=jnp.int32)
-    angles = positions.astype(F32)[:, None] * frequency[None, :]
-    cos, sin = jnp.cos(angles), jnp.sin(angles)
-    cos = jnp.concatenate([cos, cos], axis=1)
-    sin = jnp.concatenate([-sin, sin], axis=1)
+    nsp = lax.axis_size("sp")
+    frequency = ROPE_BASE ** (-np.arange(HEAD_DIM // 2) / (HEAD_DIM // 2))
+    frequency = np.tile(frequency, 2)[None, :]
+    step = np.arange(length)[:, None] * frequency
+    base = (np.arange(nsp) * length)[:, None] * frequency
+    tables = [
+        jnp.asarray(f(a).astype(np.float32)) for a in (step, base) for f in (np.cos, np.sin)
+    ]
     return tuple(
         layer(
-            lax.axis_size("sp"), lax.axis_size("tp"), tokens, query_weight, key_weight,
-            value_weight, out_weight, cos, sin, out_gain[None, :],
+            nsp, lax.axis_size("tp"), tokens, query_weight, key_weight, value_weight,
+            out_weight, tables, out_gain[None, :],
         )
     )
 

time: 77.8 us -> 76.6 us (0.985)
  other arithmetic: 1.69 us -> 0 us
    concatenate x1 -> x0, other arithmetic: 0.92 us -> none  [shards(): cos = jnp.concatenate([cos, cos], axis=1)]
where the time goes in v2:
time: 76.6 us; the launch traced here: 76.4 us
  Pallas kernels  72.5 us (95%)
  local copies, waits for them, and re-layouts  3.26 us (4%)
    pallas_call x1, Pallas kernels, layer(): pl.pallas_call(functools.partial(layer_kernel, nsp), in_specs=[hbm] * 7 +...  72.5 us
    unnamed x4, local copies, waits for them, and re-layouts  3.26 us

profile of v2, /device:TPU:1, one launch (start us, length us, event | category | flops | bytes accessed | tf_op | source)
XLA Modules:
  0.0 76.4 jit_solution(10729276638997153559)
XLA Ops:
  0.6 72.5 %layer.1 = (bf16[4,384,512]{2,1,0:T(8,128)(2,1)}, f32[4,2,384]{2,1,0:T(2,128)}) custom-call(bf16[4,384,2048]{2,1,0:T(8,128)(2,1)} %tok_h.1, bf16[2048,256]{1,0:T(8,128)(2,1)} %wq_h.1, bf16[2048,256]{1,0:T(8,128)(2,1)} %wk_h.1, bf16[2048,256]{1,0:T(8,128)(2,1)} %wv_h.1, bf16[1024,512]{1,0:T(8,128)(2,1)} %wo_h.1, f32[384,128]{1,0:T(8,128)} %constant.8.clone.cos_h, ...), custom_call_target="tpu_custom_call" | custom-call | tf_op jit(solution)/shard_map/layer/pallas_call | solution.py:513
  73.1 0.0 copy-start
  73.1 2.7 %copy.14 = bf16[4,384,512]{2,1,0:T(8,128)(2,1)} copy(bf16[4,384,512]{2,1,0:T(8,128)(2,1)} %get-tuple-element.4) | data formatting | bytes 3145728
  75.8 0.0 copy-done
  75.8 0.6 copy.15
Async XLA Ops:
  73.1 2.7 %copy-start = (f32[4,2,384]{2,1,0:T(2,128)S(1)}, f32[4,2,384]{2,1,0:T(2,128)}, u32[]{:S(2)}) copy-start(f32[4,2,384]{2,1,0:T(2,128)} %get-tuple-element.5) | copy-start | bytes 36868
